TPU v7x, 32 devices: a whole 2x2x4 slice. The times are simulated.
32 devices in a mesh: gr: 2 (over x), fs: 8 (over z, y), tp: 2 (over core).
Axes of the slice: x: 2, y: 2, z: 4, core: 2. Of those that a mesh axis runs over, the one named last changes fastest.
Arguments:
- tokens: bfloat16 [16384, 3072], P(('gr', 'fs')), may hold values from -6 to 6
- norm_gain: float32 [3072], P(('gr', 'fs')), may hold values from 0.1 to 1.9
- gate_weight: float32 [8, 3072, 768], P(None, ('gr', 'fs'), 'tp'), may hold values from -0.109375 to 0.109375
- up_weight: float32 [8, 3072, 768], P(None, ('gr', 'fs'), 'tp'), may hold values from -0.109375 to 0.109375
- down_weight: float32 [8, 3072, 768], P(None, ('gr', 'fs'), 'tp'), may hold values from -0.21875 to 0.21875
- group_pick: int32 [16384], P(('gr', 'fs')), may hold values from 0 to 3, as said below
- expert_pick: int32 [16384, 2], P(('gr', 'fs')), may hold values from 0 to 1, as said below
- route_weight: float32 [16384, 2], P(('gr', 'fs')), may hold values from 0.1 to 1
Outputs:
- combined: bfloat16 [16384, 3072], P(('gr', 'fs'), 'tp')
- gate_served: bfloat16 [8, 3072, 768], P('fs', None, 'tp')
- up_served: bfloat16 [8, 3072, 768], P('fs', None, 'tp')
- down_served: bfloat16 [8, 3072, 768], P('fs', None, 'tp')
Inputs may be any that keep to these rules, and one draw needn't show every extreme that they name: `group_pick`: in each aligned block of 1024 rows every group is picked by the same number of rows. `expert_pick`: the 2 entries of a row differ. In each aligned block of 1024 rows, every expert (group and number together) is named exactly 256 times.
All inputs are finite; a program needn't handle non-finite values.
Results may differ from a plain program's by a relative error of at most 0.0092.
Values may be sent and summed in bfloat16 or wider, within the bound.
A program may use at most 128 MiB of HBM per device.

v0:
```python
import jax
import jax.numpy as jnp
from jax import lax
from jax.sharding import PartitionSpec as P

GROUPS = 4
EPS = 1e-06


def local(
    tokens, norm_gain, gate_weight, up_weight, down_weight, group_pick, expert_pick, route_weight
):
    scaled = norm_gain[None, :, None]
    gate_local = (scaled * gate_weight).astype(jnp.bfloat16)
    up_local = (scaled * up_weight).astype(jnp.bfloat16)
    down_local = down_weight.astype(jnp.bfloat16)
    experts, rows_dev, cols_dev = gate_local.shape
    gate_four = gate_local.reshape(experts, 1, rows_dev, cols_dev)
    up_four = up_local.reshape(experts, 1, rows_dev, cols_dev)
    down_four = down_local.reshape(experts, 1, rows_dev, cols_dev)
    gathered = (
        lax.all_gather(gate_four, "gr", axis=1, tiled=True),
        lax.all_gather(up_four, "gr", axis=1, tiled=True),
        lax.all_gather(down_four, "gr", axis=1, tiled=True),
    )
    relaid = (
        lax.all_to_all(gathered[0], "fs", split_axis=0, concat_axis=2, tiled=True),
        lax.all_to_all(gathered[1], "fs", split_axis=0, concat_axis=2, tiled=True),
        lax.all_to_all(gathered[2], "fs", split_axis=0, concat_axis=2, tiled=True),
    )
    gate_new = relaid[0].reshape(1, -1, cols_dev)
    up_new = relaid[1].reshape(1, -1, cols_dev)
    down_new = relaid[2].reshape(1, -1, cols_dev)
    tok_rows, model_width = tokens.shape
    as_float = tokens.astype(jnp.float32)
    normed = (
        as_float * lax.rsqrt(jnp.mean(as_float * as_float, axis=-1, keepdims=True) + EPS)
    ).astype(jnp.bfloat16)
    per_group = experts // GROUPS
    top_count = expert_pick.shape[1]
    capacity = top_count * tok_rows // experts
    flat_ids = (group_pick[:, None] * per_group + expert_pick).reshape(-1)
    onehot = (flat_ids[:, None] == jnp.arange(experts, dtype=jnp.int32)[None, :]).astype(jnp.int32)
    slot_index = jnp.sum(onehot * (jnp.cumsum(onehot, axis=0) - 1), axis=1)
    target = flat_ids * capacity + slot_index
    source = (
        jnp.zeros((experts * capacity,), jnp.int32)
        .at[target]
        .set(jnp.arange(top_count * tok_rows, dtype=jnp.int32) // top_count)
    )
    outgoing = normed[source].reshape(experts, capacity, model_width)
    share = capacity // lax.axis_size("tp")
    start = lax.axis_index("tp") * share
    my_share = lax.dynamic_slice_in_dim(outgoing, start, share, 1)
    landed = lax.all_to_all(my_share, "fs", split_axis=0, concat_axis=1, tiled=True).reshape(
        experts, share, model_width
    )
    arrived = lax.all_gather(landed, "tp", axis=1, tiled=True).reshape(-1, model_width)
    gate_acts = jnp.dot(arrived, gate_new[0], preferred_element_type=jnp.float32)
    up_acts = jnp.dot(arrived, up_new[0], preferred_element_type=jnp.float32)
    hidden = (jax.nn.silu(gate_acts) * up_acts).astype(jnp.bfloat16)
    partial_value = lax.dot_general(
        hidden, down_new[0], (((1,), (1,)), ((), ())), preferred_element_type=jnp.float32
    ).astype(jnp.bfloat16)
    summed = (
        lax.psum_scatter(partial_value, "tp", scatter_dimension=1, tiled=True)
        .astype(jnp.float32)
        .astype(jnp.bfloat16)
    )
    returned = lax.all_to_all(summed, "fs", split_axis=0, concat_axis=0, tiled=True)
    picked = returned[target].reshape(tok_rows, top_count, -1).astype(jnp.float32)
    combined = jnp.sum(route_weight[:, :, None] * picked, axis=1).astype(jnp.bfloat16)
    return (combined, gate_new, up_new, down_new)


def solution(mesh):
    in_specs = (
        P(("gr", "fs"), None),
        P(("gr", "fs")),
        P(None, ("gr", "fs"), "tp"),
        P(None, ("gr", "fs"), "tp"),
        P(None, ("gr", "fs"), "tp"),
        P(("gr", "fs")),
        P(("gr", "fs"), None),
        P(("gr", "fs"), None),
    )
    out_specs = (
        P(("gr", "fs"), "tp"),
        P("fs", None, "tp"),
        P("fs", None, "tp"),
        P("fs", None, "tp"),
    )
    return jax.shard_map(local, mesh=mesh, in_specs=in_specs, out_specs=out_specs, check_vma=False)
```

profile of v0, /device:TPU:0, one launch (start us, length us, event | category | flops | bytes accessed | tf_op | source)
XLA Modules:
  0.0 640.0 jit_solution(4031025524227223699)
XLA Ops:
  12.8 8.0 %scatter_custom_fusion = s32[2048]{0:T(1024)S(1)} fusion(s32[2048]{0:T(1024)S(1)} %bitcast.62, s32[2048]{0:T(1024)S(1)} %add_select_fusion, s32[]{:T(128)} %constant.39.clone.1), kind=kCustom, calls=%fused_computation.34 | custom fusion | bytes 8196 | tf_op jit(solution)/shard_map/scatter | solution.py:49
  20.9 4.2 fusion
  25.5 5.1 fusion.1
  30.6 26.6 %gather_fusion = bf16[2048,3072]{1,0:T(8,128)(2,1)} fusion(bf16[1024,3072]{1,0:T(8,128)(2,1)} %fusion.1, s32[2048]{0:T(1024)S(1)} %fusion.8), kind=kCustom, calls=%fused_computation | custom fusion | bytes 25174016 | tf_op jit(solution)/shard_map/gather | solution.py:51
  57.2 5.9 constant_dynamic-slice_fusion
  63.1 7.4 %all-to-all-start = ((bf16[8,128,3072]{2,1,0:T(8,128)(2,1)}), bf16[8,128,3072]{2,1,0:T(8,128)(2,1)}, u32[]{:S(2)}, u32[]{:S(2)}) async-start(bf16[8,128,3072]{2,1,0:T(8,128)(2,1)} %constant_dynamic-slice_fusion), calls=%async_computation | async-start | bytes 12582912 | tf_op jit(solution)/shard_map/all_to_all | solution.py:55
  70.6 4.5 multiply_convert_fusion.1
  77.1 131.6 %all-to-all-done = bf16[8,128,3072]{2,1,0:T(8,128)(2,1)} async-done(((bf16[8,128,3072]{2,1,0:T(8,128)(2,1)}), bf16[8,128,3072]{2,1,0:T(8,128)(2,1)}, u32[]{:S(2)}, u32[]{:S(2)}) %all-to-all-start) | async-done | bytes 6291488 | tf_op jit(solution)/shard_map/all_to_all | solution.py:55
  208.8 3.6 all-to-all-start.1
  212.5 54.0 %all-to-all-done.1 = bf16[8,2,192,384]{3,2,1,0:T(8,128)(2,1)S(1)} async-done(((bf16[8,2,192,384]{3,2,1,0:T(8,128)(2,1)}), bf16[8,2,192,384]{3,2,1,0:T(8,128)(2,1)S(1)}, u32[]{:S(2)}, u32[]{:S(2)}) %all-to-all-start.1) | async-done | bytes 2359328 | tf_op jit(solution)/shard_map/all_to_all | solution.py:27
  266.5 4.4 all-to-all-start.2
  270.9 53.4 %all-to-all-done.2 = bf16[8,2,192,384]{3,2,1,0:T(8,128)(2,1)} async-done(((bf16[8,2,192,384]{3,2,1,0:T(8,128)(2,1)}), bf16[8,2,192,384]{3,2,1,0:T(8,128)(2,1)}, u32[]{:S(2)}, u32[]{:S(2)}) %all-to-all-start.2) | async-done | bytes 2359328 | tf_op jit(solution)/shard_map/all_to_all | solution.py:28
  324.3 4.4 all-to-all-start.3
  330.6 3.3 copy.32
  333.9 48.2 %all-to-all-done.3 = bf16[8,2,192,384]{3,2,1,0:T(8,128)(2,1)} async-done(((bf16[8,2,192,384]{3,2,1,0:T(8,128)(2,1)}), bf16[8,2,192,384]{3,2,1,0:T(8,128)(2,1)}, u32[]{:S(2)}, u32[]{:S(2)}) %all-to-all-start.3) | async-done | bytes 2359328 | tf_op jit(solution)/shard_map/all_to_all | solution.py:29
  382.1 3.3 copy.33
  385.4 10.7 %fusion.13 = f32[2048,384]{1,0:T(8,128)} fusion(bf16[2048,3072]{1,0:T(8,128)(2,1)} %bitcast.65, bf16[3072,384]{1,0:T(8,128)(2,1)S(1)} %bitcast.54), kind=kOutput, calls=%fused_computation.40 | convolution fusion | flops 4831838208 | bytes 18087936 | tf_op jit(solution)/shard_map/dot_general | solution.py:59
  396.1 20.7 %convolution_convert_fusion = bf16[2048,3072]{1,0:T(8,128)(2,1)} fusion(bf16[3072,384]{1,0:T(8,128)(2,1)} %bitcast.59, f32[2048,384]{1,0:T(8,128)} %fusion.13, bf16[2048,3072]{1,0:T(8,128)(2,1)} %bitcast.66, bf16[3072,384]{1,0:T(8,128)(2,1)} %bitcast.55), kind=kOutput, calls=%fused_computation.8 | convolution fusion | flops 9674686464 | bytes 33030144 | tf_op jit(solution)/shard_map/dot_general | solution.py:62
  416.9 18.6 %reduce-scatter.2.cloned.1.call-done = bf16[2048,1536]{1,0:T(8,128)(2,1)} async-done(((bf16[2048,3072]{1,0:T(8,128)(2,1)}), bf16[2048,1536]{1,0:T(8,128)(2,1)}) %reduce-scatter.2.cloned.1.call-update) | async-done | bytes 6291472 | tf_op jit(solution)/shard_map/reduce_scatter | solution.py:66
  435.5 6.0 all-to-all-start.4
  441.7 138.3 %all-to-all-done.4 = bf16[8,256,1536]{2,1,0:T(8,128)(2,1)} async-done(((bf16[8,256,1536]{2,1,0:T(8,128)(2,1)}), bf16[8,256,1536]{2,1,0:T(8,128)(2,1)}, u32[]{:S(2)}, u32[]{:S(2)}) %all-to-all-start.4) | async-done | bytes 6291488 | tf_op jit(solution)/shard_map/all_to_all | solution.py:70
  580.0 16.9 %gather_fusion.1 = bf16[2048,1536]{1,0:T(8,128)(2,1)} fusion(bf16[2048,1536]{1,0:T(8,128)(2,1)} %bitcast.18, s32[2048]{0:T(1024)S(1)} %broadcast_clamp_fusion), kind=kCustom, calls=%fused_computation.1 | custom fusion | bytes 12591104 | tf_op jit(solution)/shard_map/gather | solution.py:71
  596.9 14.2 %reshape.117 = f32[1024,2,1536]{2,1,0:T(2,128)} reshape(bf16[2048,1536]{1,0:T(8,128)(2,1)} %gather_fusion.1) | data formatting | bytes 18874368 | tf_op jit(solution)/shard_map/convert_element_type | solution.py:71
  611.1 22.4 %multiply_reduce_fusion = bf16[1024,1536]{1,0:T(8,128)(2,1)} fusion(f32[1024,2,1536]{2,1,0:T(2,128)} %reshape.117, f32[1024,2]{1,0:T(8,128)S(1)} %copy.27), kind=kLoop, calls=%fused_computation.7 | loop fusion | flops 4718592 | bytes 15736832 | tf_op jit(solution)/shard_map/reduce_sum | solution.py:72
  (45 shorter events, 10.2 us)
Async XLA Ops:
  20.9 4.6 copy-start
  63.1 7.5 %copy-start.4 = (f32[192]{0:T(256)S(1)}, f32[192]{0:T(256)}, u32[]{:S(2)}) copy-start(f32[192]{0:T(256)} %param.9) | copy-start | bytes 2308
  63.1 145.7 %all-to-all-start = ((bf16[8,128,3072]{2,1,0:T(8,128)(2,1)}), bf16[8,128,3072]{2,1,0:T(8,128)(2,1)}, u32[]{:S(2)}, u32[]{:S(2)}) async-start(bf16[8,128,3072]{2,1,0:T(8,128)(2,1)} %constant_dynamic-slice_fusion), calls=%async_computation | async-start | bytes 12582912 | tf_op jit(solution)/shard_map/all_to_all | solution.py:55
  70.5 5.4 copy-start.1
  70.5 138.3 %all-gather.10.cloned.1.call-start = ((), (), s32[]{:S(2)}) async-start(), calls=%async_computation.8 | async-start | bytes 3538944 | tf_op jit(solution)/shard_map/all_gather | solution.py:22
  75.1 137.4 %all-gather.12.cloned.1.call-start = ((), (), s32[]{:S(2)}) async-start(), calls=%async_computation.9 | async-start | bytes 3538944 | tf_op jit(solution)/shard_map/all_gather | solution.py:23
  75.9 195.0 %all-gather.14.cloned.1.call-start = ((), (), s32[]{:S(2)}) async-start(), calls=%async_computation.10 | async-start | bytes 3538944 | tf_op jit(solution)/shard_map/all_gather | solution.py:24
  77.1 308.3 %all-gather.8.cloned.1.call-start = ((), (), s32[]{:S(2)}) async-start(), calls=%async_computation.6 | async-start | bytes 18874368 | tf_op jit(solution)/shard_map/all_gather | solution.py:58
  208.8 57.7 %all-to-all-start.1 = ((bf16[8,2,192,384]{3,2,1,0:T(8,128)(2,1)}), bf16[8,2,192,384]{3,2,1,0:T(8,128)(2,1)S(1)}, u32[]{:S(2)}, u32[]{:S(2)}) async-start(bf16[8,2,192,384]{3,2,1,0:T(8,128)(2,1)} %bitcast.58), calls=%async_computation.1 | async-start | bytes 4718592 | tf_op jit(solution)/shard_map/all_to_all | solution.py:27
  266.5 57.8 %all-to-all-start.2 = ((bf16[8,2,192,384]{3,2,1,0:T(8,128)(2,1)}), bf16[8,2,192,384]{3,2,1,0:T(8,128)(2,1)}, u32[]{:S(2)}, u32[]{:S(2)}) async-start(bf16[8,2,192,384]{3,2,1,0:T(8,128)(2,1)} %bitcast.57), calls=%async_computation.2 | async-start | bytes 4718592 | tf_op jit(solution)/shard_map/all_to_all | solution.py:28
  324.3 57.8 %all-to-all-start.3 = ((bf16[8,2,192,384]{3,2,1,0:T(8,128)(2,1)}), bf16[8,2,192,384]{3,2,1,0:T(8,128)(2,1)}, u32[]{:S(2)}, u32[]{:S(2)}) async-start(bf16[8,2,192,384]{3,2,1,0:T(8,128)(2,1)} %bitcast.52), calls=%async_computation.3 | async-start | bytes 4718592 | tf_op jit(solution)/shard_map/all_to_all | solution.py:29
  328.7 106.8 %reduce-scatter.2.cloned.1.call-start = ((), (), s32[]{:S(2)}) async-start(), calls=%async_computation.7 | async-start | bytes 18874368 | tf_op jit(solution)/shard_map/reduce_scatter | solution.py:66
  333.9 51.5 %copy-start.2 = (bf16[8,2,192,384]{3,2,0,1:T(8,128)(2,1)S(1)}, bf16[8,2,192,384]{3,2,0,1:T(8,128)(2,1)}, u32[]{:S(2)}) copy-start(bf16[8,2,192,384]{3,2,0,1:T(8,128)(2,1)} %copy.31) | copy-start | bytes 7077892
  435.4 6.0 copy-start.3
  435.5 144.6 %all-to-all-start.4 = ((bf16[8,256,1536]{2,1,0:T(8,128)(2,1)}), bf16[8,256,1536]{2,1,0:T(8,128)(2,1)}, u32[]{:S(2)}, u32[]{:S(2)}) async-start(bf16[8,256,1536]{2,1,0:T(8,128)(2,1)} %bitcast.51), calls=%async_computation.5 | async-start | bytes 12582912 | tf_op jit(solution)/shard_map/all_to_all | solution.py:70
Sparse Core Ops, SparseCore 0:
  75.2 37.3 all-gather.9
  114.8 36.0 all-gather.11
  153.0 36.0 all-gather.13
  208.9 23.5 all-gather.7
  417.0 18.4 reduce-scatter.1
where the time goes:
time: 641 us; the launch traced here: 640 us
  waiting for transfers between devices  445 us (69%)
  local copies, waits for them, and re-layouts  82.1 us (13%)
  other arithmetic  41.4 us (6%)
  matrix products  31.4 us (5%)
  starting transfers between devices  26.3 us (4%)
  between operations  14 us (2%)
    all_to_all x1, waiting for transfers between devices, local(): lax.all_to_all(summed, 'fs', split_axis=0, concat_axis=0, tiled=True)  138 us
    all_to_all x1, waiting for transfers between devices, local(): lax.all_to_all(my_share, 'fs', split_axis=0, concat_axis=1, tiled=True)  132 us
    all_to_all x1, waiting for transfers between devices, local(): lax.all_to_all(gathered[0], 'fs', split_axis=0, concat_axis=2, tiled=True)  54 us
    all_to_all x1, waiting for transfers between devices, local(): lax.all_to_all(gathered[1], 'fs', split_axis=0, concat_axis=2, tiled=True)  53.4 us
    all_to_all x1, waiting for transfers between devices, local(): lax.all_to_all(gathered[2], 'fs', split_axis=0, concat_axis=2, tiled=True)  48.2 us
    gather x1, local copies, waits for them, and re-layouts, local(): outgoing = normed[source].reshape(experts, capacity, model_width)  26.6 us
    reduce_sum x1, other arithmetic, local(): jnp.sum(route_weight[:, :, None] * picked, axis=1).astype(jnp.bfloat16)  22.4 us
    dot_general x1, matrix products, local(): lax.dot_general(hidden, down_new[0], (((1,), (1,)), ((), ())), preferred_...  20.7 us
  transfers between devices with their start and end apart: 10, of which 6 were waited for; matrix products, arithmetic and copies ran while one was open for 2% of the time, Pallas kernels for 0%

commit v1 on v0

--- a/solution.py
+++ b/solution.py
@@ -10,6 +10,28 @@
 def local(
     tokens, norm_gain, gate_weight, up_weight, down_weight, group_pick, expert_pick, route_weight
 ):
+
+    def proceed_the_sites(buf, along_dim, array_axis):
+        carry_in = jax.lax.axis_size("fs")
+        after = jax.lax.axis_index("fs")
+        local_now, main = (carry_in, after)
+        val = buf.shape[along_dim] // local_now
+        value_now = list(buf.shape)
+        value_now[along_dim] = val
+        tile_out = value_now[array_axis]
+        value_now[array_axis] = tile_out * local_now
+        v_now = jnp.zeros(value_now, buf.dtype)
+        for i in range(local_now):
+            piece_out = lax.dynamic_slice_in_dim(buf, (main ^ i) * val, val, axis=along_dim)
+            if i:
+                piece_out = jax.lax.ppermute(
+                    piece_out, "fs", [(k0, k0 ^ i) for k0 in range(local_now)]
+                )
+            v_now = lax.dynamic_update_slice_in_dim(
+                v_now, piece_out, (main ^ i) * tile_out, axis=array_axis
+            )
+        return v_now
+
     scaled = norm_gain[None, :, None]
     gate_local = (scaled * gate_weight).astype(jnp.bfloat16)
     up_local = (scaled * up_weight).astype(jnp.bfloat16)
@@ -26,7 +48,7 @@
     relaid = (
         lax.all_to_all(gathered[0], "fs", split_axis=0, concat_axis=2, tiled=True),
         lax.all_to_all(gathered[1], "fs", split_axis=0, concat_axis=2, tiled=True),
-        lax.all_to_all(gathered[2], "fs", split_axis=0, concat_axis=2, tiled=True),
+        proceed_the_sites(gathered[2], along_dim=0, array_axis=2),
     )
     gate_new = relaid[0].reshape(1, -1, cols_dev)
     up_new = relaid[1].reshape(1, -1, cols_dev)

time: 641 us -> 636 us (level)
  waiting for transfers between devices: 445 us -> 419 us
  starting transfers between devices: 26.3 us -> 38.7 us
  local copies, waits for them, and re-layouts: 82.1 us -> 91.5 us
    ppermute x0 -> x7, waiting for transfers between devices: none -> 66.4 us  [proceed_the_sites(): jax.lax.ppermute(piece_out, 'fs', [(k0, k0 ^ i) for k0 in range(local_now)])]
    all_to_all x1, waiting for transfers between devices: 53.4 us -> 0.01 us  [local(): lax.all_to_all(gathered[1], 'fs', split_axis=0, concat_axis=2, tiled=True)]
    all_to_all x1 -> x0, waiting for transfers between devices: 48.2 us -> none  [local(): lax.all_to_all(gathered[2], 'fs', split_axis=0, concat_axis=2, tiled=True)]
    ppermute x0 -> x7, starting transfers between devices: none -> 16.8 us  [proceed_the_sites(): jax.lax.ppermute(piece_out, 'fs', [(k0, k0 ^ i) for k0 in range(local_now)])]
    reduce_scatter x1, waiting for transfers between devices: 18.6 us -> 27.7 us  [local(): lax.psum_scatter(partial_value, 'tp', scatter_dimension=1, tiled=True)]
    dynamic_update_slice x0 -> x7, local copies, waits for them, and re-layouts: none -> 8.08 us  [proceed_the_sites(): lax.dynamic_update_slice_in_dim(v_now, piece_out, (main ^ i) * tile_out,...]
  transfers between devices with their start and end apart: 10 -> 16, of which waited for: 6 -> 9; matrix products, arithmetic and copies ran while one was open for 2% -> 3% of each run, Pallas kernels for 0% -> 0%
where the time goes in v1:
time: 636 us; the launch traced here: 635 us
  waiting for transfers between devices  419 us (66%)
  local copies, waits for them, and re-layouts  91.5 us (14%)
  other arithmetic  40.5 us (6%)
  starting transfers between devices  38.7 us (6%)
  matrix products  31.4 us (5%)
  between operations  14 us (2%)
    all_to_all x1, waiting for transfers between devices, local(): lax.all_to_all(summed, 'fs', split_axis=0, concat_axis=0, tiled=True)  138 us
    all_to_all x1, waiting for transfers between devices, local(): lax.all_to_all(my_share, 'fs', split_axis=0, concat_axis=1, tiled=True)  132 us
    ppermute x7, waiting for transfers between devices, proceed_the_sites(): jax.lax.ppermute(piece_out, 'fs', [(k0, k0 ^ i) for k0 in range(local_now)])  66.4 us
    all_to_all x1, waiting for transfers between devices, local(): lax.all_to_all(gathered[0], 'fs', split_axis=0, concat_axis=2, tiled=True)  54 us
    reduce_scatter x1, waiting for transfers between devices, local(): lax.psum_scatter(partial_value, 'tp', scatter_dimension=1, tiled=True)  27.7 us
    gather x1, local copies, waits for them, and re-layouts, local(): outgoing = normed[source].reshape(experts, capacity, model_width)  26.6 us
    reduce_sum x1, other arithmetic, local(): jnp.sum(route_weight[:, :, None] * picked, axis=1).astype(jnp.bfloat16)  22.4 us
    dot_general x1, matrix products, local(): lax.dot_general(hidden, down_new[0], (((1,), (1,)), ((), ())), preferred_...  20.7 us
  transfers between devices with their start and end apart: 16, of which 9 were waited for; matrix products, arithmetic and copies ran while one was open for 3% of the time, Pallas kernels for 0%

profile of v1, /device:TPU:0, one launch (start us, length us, event | category | flops | bytes accessed | tf_op | source)
XLA Modules:
  0.0 635.2 jit_solution(11858004120499704359)
XLA Ops:
  12.8 8.0 %scatter_custom_fusion = s32[2048]{0:T(1024)S(1)} fusion(s32[2048]{0:T(1024)S(1)} %bitcast.55, s32[2048]{0:T(1024)S(1)} %add_select_fusion, s32[]{:T(128)} %constant.26.clone.1), kind=kCustom, calls=%fused_computation.50 | custom fusion | bytes 8196 | tf_op jit(solution)/shard_map/scatter | solution.py:71
  20.9 4.2 fusion
  25.5 5.1 fusion.1
  30.6 26.6 %gather_fusion = bf16[2048,3072]{1,0:T(8,128)(2,1)} fusion(bf16[1024,3072]{1,0:T(8,128)(2,1)} %fusion.1, s32[2048]{0:T(1024)S(1)} %fusion.8), kind=kCustom, calls=%fused_computation | custom fusion | bytes 25174016 | tf_op jit(solution)/shard_map/gather | solution.py:73
  57.2 5.9 constant_dynamic-slice_fusion.7
  63.1 7.4 %all-to-all-start = ((bf16[8,128,3072]{2,1,0:T(8,128)(2,1)}), bf16[8,128,3072]{2,1,0:T(8,128)(2,1)}, u32[]{:S(2)}, u32[]{:S(2)}) async-start(bf16[8,128,3072]{2,1,0:T(8,128)(2,1)} %constant_dynamic-slice_fusion.7), calls=%async_computation | async-start | bytes 12582912 | tf_op jit(solution)/shard_map/all_to_all | solution.py:77
  77.1 131.7 %all-to-all-done = bf16[8,128,3072]{2,1,0:T(8,128)(2,1)} async-done(((bf16[8,128,3072]{2,1,0:T(8,128)(2,1)}), bf16[8,128,3072]{2,1,0:T(8,128)(2,1)}, u32[]{:S(2)}, u32[]{:S(2)}) %all-to-all-start) | async-done | bytes 6291488 | tf_op jit(solution)/shard_map/all_to_all | solution.py:77
  208.8 3.6 all-to-all-start.1
  212.5 54.0 %all-to-all-done.1 = bf16[8,2,192,384]{3,2,1,0:T(8,128)(2,1)S(1)} async-done(((bf16[8,2,192,384]{3,2,1,0:T(8,128)(2,1)}), bf16[8,2,192,384]{3,2,1,0:T(8,128)(2,1)S(1)}, u32[]{:S(2)}, u32[]{:S(2)}) %all-to-all-start.1) | async-done | bytes 2359328 | tf_op jit(solution)/shard_map/all_to_all | solution.py:49
  266.5 4.4 all-to-all-start.2
  282.3 15.0 %collective-permute-done = bf16[1,2,192,384]{3,2,1,0:T(8,128)(2,1)} collective-permute-done((bf16[1,2,192,384]{3,2,1,0:T(8,128)(2,1)}, bf16[1,2,192,384]{3,2,1,0:T(8,128)(2,1)}, u32[]{:S(2)}, u32[]{:S(2)}) %collective-permute-start) | collective-permute-done | bytes 294944 | tf_op jit(solution)/shard_map/ppermute | solution.py:27
  297.3 5.5 collective-permute-start.5
  304.5 12.8 %collective-permute-done.1 = bf16[1,2,192,384]{3,2,1,0:T(8,128)(2,1)} collective-permute-done((bf16[1,2,192,384]{3,2,1,0:T(8,128)(2,1)}, bf16[1,2,192,384]{3,2,1,0:T(8,128)(2,1)}, u32[]{:S(2)}, u32[]{:S(2)}) %collective-permute-start.1) | collective-permute-done | bytes 294944 | tf_op jit(solution)/shard_map/ppermute | solution.py:27
  317.3 3.9 collective-permute-start.6
  325.4 32.2 %collective-permute-done.3 = bf16[1,2,192,384]{3,2,1,0:T(8,128)(2,1)S(1)} collective-permute-done((bf16[1,2,192,384]{3,2,1,0:T(8,128)(2,1)S(1)}, bf16[1,2,192,384]{3,2,1,0:T(8,128)(2,1)S(1)}, u32[]{:S(2)}, u32[]{:S(2)}) %collective-permute-start.3) | collective-permute-done | bytes 294944 | tf_op jit(solution)/shard_map/ppermute | solution.py:27
  358.4 5.7 collective-permute-done.4
  371.4 10.7 %fusion.13 = f32[2048,384]{1,0:T(8,128)} fusion(bf16[2048,3072]{1,0:T(8,128)(2,1)} %bitcast.58, bf16[3072,384]{1,0:T(8,128)(2,1)S(1)} %bitcast.50), kind=kOutput, calls=%fused_computation.55 | convolution fusion | flops 4831838208 | bytes 18087936 | tf_op jit(solution)/shard_map/dot_general | solution.py:81
  382.2 20.7 %convolution_convert_fusion = bf16[2048,3072]{1,0:T(8,128)(2,1)} fusion(bf16[3072,384]{1,0:T(8,128)(2,1)} %bitcast.14, f32[2048,384]{1,0:T(8,128)} %fusion.13, bf16[2048,3072]{1,0:T(8,128)(2,1)} %bitcast.59, bf16[3072,384]{1,0:T(8,128)(2,1)} %bitcast.52), kind=kOutput, calls=%fused_computation.8 | convolution fusion | flops 9674686464 | bytes 33030144 | tf_op jit(solution)/shard_map/dot_general | solution.py:84
  402.9 27.7 %reduce-scatter.2.cloned.1.call-done = bf16[2048,1536]{1,0:T(8,128)(2,1)} async-done(((bf16[2048,3072]{1,0:T(8,128)(2,1)}), bf16[2048,1536]{1,0:T(8,128)(2,1)}) %reduce-scatter.2.cloned.1.call-update) | async-done | bytes 6291472 | tf_op jit(solution)/shard_map/reduce_scatter | solution.py:88
  430.6 6.0 all-to-all-start.3
  436.9 138.3 %all-to-all-done.3 = bf16[8,256,1536]{2,1,0:T(8,128)(2,1)} async-done(((bf16[8,256,1536]{2,1,0:T(8,128)(2,1)}), bf16[8,256,1536]{2,1,0:T(8,128)(2,1)}, u32[]{:S(2)}, u32[]{:S(2)}) %all-to-all-start.3) | async-done | bytes 6291488 | tf_op jit(solution)/shard_map/all_to_all | solution.py:92
  575.2 16.9 %gather_fusion.1 = bf16[2048,1536]{1,0:T(8,128)(2,1)} fusion(bf16[2048,1536]{1,0:T(8,128)(2,1)} %bitcast.16, s32[2048]{0:T(1024)S(1)} %broadcast_clamp_fusion), kind=kCustom, calls=%fused_computation.1 | custom fusion | bytes 12591104 | tf_op jit(solution)/shard_map/gather | solution.py:93
  592.1 14.2 %reshape.115 = f32[1024,2,1536]{2,1,0:T(2,128)} reshape(bf16[2048,1536]{1,0:T(8,128)(2,1)} %gather_fusion.1) | data formatting | bytes 18874368 | tf_op jit(solution)/shard_map/convert_element_type | solution.py:93
  606.3 22.4 %multiply_reduce_fusion = bf16[1024,1536]{1,0:T(8,128)(2,1)} fusion(f32[1024,2,1536]{2,1,0:T(2,128)} %reshape.115, f32[1024,2]{1,0:T(8,128)S(1)} %copy.25), kind=kLoop, calls=%fused_computation.7 | loop fusion | flops 4718592 | bytes 15736832 | tf_op jit(solution)/shard_map/reduce_sum | solution.py:94
  (69 shorter events, 38.1 us)
Async XLA Ops:
  20.9 4.6 copy-start
  63.1 7.5 %copy-start.4 = (f32[8,192,384]{2,1,0:T(8,128)S(1)}, f32[8,192,384]{2,1,0:T(8,128)}, u32[]{:S(2)}) copy-start(f32[8,192,384]{2,1,0:T(8,128)} %param.11) | copy-start | bytes 7077892
  63.1 7.5 %copy-start.6 = (f32[192]{0:T(256)S(1)}, f32[192]{0:T(256)}, u32[]{:S(2)}) copy-start(f32[192]{0:T(256)} %param.9) | copy-start | bytes 2308
  63.1 145.7 %all-to-all-start = ((bf16[8,128,3072]{2,1,0:T(8,128)(2,1)}), bf16[8,128,3072]{2,1,0:T(8,128)(2,1)}, u32[]{:S(2)}, u32[]{:S(2)}) async-start(bf16[8,128,3072]{2,1,0:T(8,128)(2,1)} %constant_dynamic-slice_fusion.7), calls=%async_computation | async-start | bytes 12582912 | tf_op jit(solution)/shard_map/all_to_all | solution.py:77
  70.5 138.3 %all-gather.10.cloned.1.call-start = ((), (), s32[]{:S(2)}) async-start(), calls=%async_computation.7 | async-start | bytes 3538944 | tf_op jit(solution)/shard_map/all_gather | solution.py:44
  74.2 1.7 copy-start.1
  74.2 138.2 %all-gather.12.cloned.1.call-start = ((), (), s32[]{:S(2)}) async-start(), calls=%async_computation.8 | async-start | bytes 3538944 | tf_op jit(solution)/shard_map/all_gather | solution.py:45
  75.0 196.2 %all-gather.14.cloned.1.call-start = ((), (), s32[]{:S(2)}) async-start(), calls=%async_computation.9 | async-start | bytes 3538944 | tf_op jit(solution)/shard_map/all_gather | solution.py:46
  77.1 294.3 %all-gather.8.cloned.1.call-start = ((), (), s32[]{:S(2)}) async-start(), calls=%async_computation.5 | async-start | bytes 18874368 | tf_op jit(solution)/shard_map/all_gather | solution.py:80
  208.8 57.7 %all-to-all-start.1 = ((bf16[8,2,192,384]{3,2,1,0:T(8,128)(2,1)}), bf16[8,2,192,384]{3,2,1,0:T(8,128)(2,1)S(1)}, u32[]{:S(2)}, u32[]{:S(2)}) async-start(bf16[8,2,192,384]{3,2,1,0:T(8,128)(2,1)} %bitcast.51), calls=%async_computation.1 | async-start | bytes 4718592 | tf_op jit(solution)/shard_map/all_to_all | solution.py:49
  266.5 101.4 %all-to-all-start.2 = ((bf16[8,2,192,384]{3,2,1,0:T(8,128)(2,1)}), bf16[8,2,192,384]{3,2,1,0:T(8,128)(2,1)}, u32[]{:S(2)}, u32[]{:S(2)}) async-start(bf16[8,2,192,384]{3,2,1,0:T(8,128)(2,1)} %bitcast.47), calls=%async_computation.2 | async-start | bytes 4718592 | tf_op jit(solution)/shard_map/all_to_all | solution.py:50
  270.9 159.7 %reduce-scatter.2.cloned.1.call-start = ((), (), s32[]{:S(2)}) async-start(), calls=%async_computation.6 | async-start | bytes 18874368 | tf_op jit(solution)/shard_map/reduce_scatter | solution.py:88
  271.2 2.5 copy-start.2
  274.9 22.4 %collective-permute-start = (bf16[1,2,192,384]{3,2,1,0:T(8,128)(2,1)}, bf16[1,2,192,384]{3,2,1,0:T(8,128)(2,1)}, u32[]{:S(2)}, u32[]{:S(2)}) collective-permute-start(bf16[1,2,192,384]{3,2,1,0:T(8,128)(2,1)} %get-tuple-element.12), channel_id=1, source_target_pairs={{0,2},{2,0},{4,6},{6,4},{8,10},{10,8},{12,14},{14,12},{1,3},{3,1},... | collective-permute-start | bytes 884744 | tf_op jit(solution)/shard_map/ppermute | solution.py:27
  276.5 40.9 %collective-permute-start.1 = (bf16[1,2,192,384]{3,2,1,0:T(8,128)(2,1)}, bf16[1,2,192,384]{3,2,1,0:T(8,128)(2,1)}, u32[]{:S(2)}, u32[]{:S(2)}) collective-permute-start(bf16[1,2,192,384]{3,2,1,0:T(8,128)(2,1)} %get-tuple-element.11), channel_id=1, source_target_pairs={{0,4},{2,6},{4,0},{6,2},{8,12},{10,14},{12,8},{14,10},{1,5},{3,7},... | collective-permute-start | bytes 884744 | tf_op jit(solution)/shard_map/ppermute | solution.py:27
  278.0 45.7 %collective-permute-start.2 = (bf16[1,2,192,384]{3,2,1,0:T(8,128)(2,1)}, bf16[1,2,192,384]{3,2,1,0:T(8,128)(2,1)}, u32[]{:S(2)}, u32[]{:S(2)}) collective-permute-start(bf16[1,2,192,384]{3,2,1,0:T(8,128)(2,1)} %get-tuple-element.10), channel_id=1, source_target_pairs={{0,6},{2,4},{4,2},{6,0},{8,14},{10,12},{12,10},{14,8},{1,7},{3,5},... | collective-permute-start | bytes 884744 | tf_op jit(solution)/shard_map/ppermute | solution.py:27
  278.4 79.2 %collective-permute-start.3 = (bf16[1,2,192,384]{3,2,1,0:T(8,128)(2,1)S(1)}, bf16[1,2,192,384]{3,2,1,0:T(8,128)(2,1)S(1)}, u32[]{:S(2)}, u32[]{:S(2)}) collective-permute-start(bf16[1,2,192,384]{3,2,1,0:T(8,128)(2,1)S(1)} %get-tuple-element.9), channel_id=1, source_target_pairs={{0,8},{2,10},{4,12},{6,14},{8,0},{10,2},{12,4},{14,6},{1,9},{3,11}... | collective-permute-start | bytes 884744 | tf_op jit(solution)/shard_map/ppermute | solution.py:27
  280.9 83.1 %collective-permute-start.4 = (bf16[1,2,192,384]{3,2,1,0:T(8,128)(2,1)S(1)}, bf16[1,2,192,384]{3,2,1,0:T(8,128)(2,1)S(1)}, u32[]{:S(2)}, u32[]{:S(2)}) collective-permute-start(bf16[1,2,192,384]{3,2,1,0:T(8,128)(2,1)S(1)} %get-tuple-element.8), channel_id=1, source_target_pairs={{0,10},{2,8},{4,14},{6,12},{8,2},{10,0},{12,6},{14,4},{1,11},{3,9}... | collective-permute-start | bytes 884744 | tf_op jit(solution)/shard_map/ppermute | solution.py:27
  297.3 67.5 %collective-permute-start.5 = (bf16[1,2,192,384]{3,2,1,0:T(8,128)(2,1)S(1)}, bf16[1,2,192,384]{3,2,1,0:T(8,128)(2,1)S(1)}, u32[]{:S(2)}, u32[]{:S(2)}) collective-permute-start(bf16[1,2,192,384]{3,2,1,0:T(8,128)(2,1)S(1)} %get-tuple-element.7), channel_id=1, source_target_pairs={{0,12},{2,14},{4,8},{6,10},{8,4},{10,6},{12,0},{14,2},{1,13},{3,15... | collective-permute-start | bytes 884744 | tf_op jit(solution)/shard_map/ppermute | solution.py:27
  317.3 48.2 %collective-permute-start.6 = (bf16[1,2,192,384]{3,2,1,0:T(8,128)(2,1)S(1)}, bf16[1,2,192,384]{3,2,1,0:T(8,128)(2,1)S(1)}, u32[]{:S(2)}, u32[]{:S(2)}) collective-permute-start(bf16[1,2,192,384]{3,2,1,0:T(8,128)(2,1)S(1)} %get-tuple-element.6), channel_id=1, source_target_pairs={{0,14},{2,12},{4,10},{6,8},{8,6},{10,4},{12,2},{14,0},{1,15},{3,13... | collective-permute-start | bytes 884744 | tf_op jit(solution)/shard_map/ppermute | solution.py:27
  367.9 3.5 copy-start.3
  430.6 6.0 copy-start.5
  430.6 144.6 %all-to-all-start.3 = ((bf16[8,256,1536]{2,1,0:T(8,128)(2,1)}), bf16[8,256,1536]{2,1,0:T(8,128)(2,1)}, u32[]{:S(2)}, u32[]{:S(2)}) async-start(bf16[8,256,1536]{2,1,0:T(8,128)(2,1)} %bitcast.46), calls=%async_computation.4 | async-start | bytes 12582912 | tf_op jit(solution)/shard_map/all_to_all | solution.py:92
Sparse Core Ops, SparseCore 0:
  74.4 37.3 all-gather.9
  113.9 36.0 all-gather.11
  152.1 36.0 all-gather.13
  208.9 23.5 all-gather.7
  403.0 27.5 reduce-scatter.1
